TPU v7x, 32 devices: a whole 2x2x4 slice. The times are simulated.
32 devices in a mesh: sp: 8 (over z, y), tp: 4 (over x, core).
Axes of the slice: x: 2, y: 2, z: 4, core: 2. Of those that a mesh axis runs over, the one named last changes fastest.
Arguments:
- resid: bfloat16 [2048, 2048], P(('sp', 'tp')), may hold values from -6 to 6
- mix_in: bfloat16 [2048, 512], P('sp', 'tp'), may hold values from -6 to 6
- decay_rate: float32 [32, 64], P('tp'), may hold values from -0.05 to 0, as said below
- turn_rate: float32 [32, 64], P('tp'), may hold values from -3.140625 to 3.140625
- forget: float32 [2048, 32], P('sp', 'tp'), may hold values from -2 to 0, as said below
- input_real: float32 [32, 64, 16], P('tp'), may hold values from -1 to 1
- input_imag: float32 [32, 64, 16], P('tp'), may hold values from -1 to 1
- output_real: float32 [32, 16, 64], P('tp'), may hold values from -0.75 to 0.75
- output_imag: float32 [32, 16, 64], P('tp'), may hold values from -0.75 to 0.75
- skip_gain: float32 [32, 16], P('tp'), may hold values from -5 to 5
- mix_gain: float32 [512], replicated, may hold values from 0.1 to 1.9
- w_out: bfloat16 [512, 2048], replicated, may hold values from -0.25 to 0.25
- ffn_gain: float32 [2048], replicated, may hold values from 0.1 to 1.9
- gating_matrix: bfloat16 [2048, 5632], P('sp', 'tp'), may hold values from -0.125 to 0.125
- w_up: bfloat16 [2048, 5632], P('sp', 'tp'), may hold values from -0.125 to 0.125
- w_down: bfloat16 [5632, 2048], P('tp', 'sp'), may hold values from -0.078125 to 0.078125
Outputs:
- result: bfloat16 [2048, 2048], P(('sp', 'tp'))
Inputs may be any that keep to these rules, and one draw needn't show every extreme that they name: `decay_rate`: every entry is negative. `forget`: every entry is at most zero.
All inputs are finite; a program needn't handle non-finite values.
Results may differ from a plain program's by a relative error of at most 0.012.
Values may be sent and summed in bfloat16 or wider, within the bound.
A program may use at most 128 MiB of HBM per device.

v0:
```python
import jax
import jax.numpy as jnp
from jax import lax
from jax.sharding import PartitionSpec as P

eps = 1e-06


def carried_in(part, axis, combine, identity):
    place = lax.axis_index(axis)
    gathered = jax.tree.map(lambda a: lax.all_gather(a, axis), part)
    state = jax.tree.map(lambda a, e: jnp.zeros_like(a) + jnp.asarray(e, a.dtype), part, identity)

    def one(turn, state):
        return combine(
            state, jax.tree.map(lambda a: lax.dynamic_index_in_dim(a, turn, 0, False), gathered)
        )

    return lax.fori_loop(0, place, one, state)


def chain(earlier, later):
    first_real, first_imag, push_real, push_imag = earlier
    next_real, next_imag, add_real, add_imag = later
    return (
        next_real * first_real - next_imag * first_imag,
        next_real * first_imag + next_imag * first_real,
        next_real * push_real - next_imag * push_imag + add_real,
        next_real * push_imag + next_imag * push_real + add_imag,
    )


def local_states(log_step, push_real, push_imag, turn):
    high = lax.Precision.HIGHEST
    n_rows, columns = log_step.shape
    span = min(32, n_rows)
    n_spans = n_rows // span
    place = jnp.arange(span, dtype=jnp.float32)
    lower = place[:, None] >= place[None, :]
    lower_cube = lower[:, :, None]
    triangle = lower.astype(jnp.float32)
    lag_angle = (place[:, None] - place[None, :])[:, :, None] * turn[None, None, :]
    lag_cos = jnp.where(lower_cube, jnp.cos(lag_angle), 0.0)
    lag_sin = jnp.where(lower_cube, jnp.sin(lag_angle), 0.0)
    ahead = place + 1.0
    own_cos = jnp.cos(ahead[:, None] * turn[None, :])
    own_sin = jnp.sin(ahead[:, None] * turn[None, :])

    def advance(carry, blocks):
        run_log, state_real, state_imag, offset = carry
        log_block, real_block, imag_block = blocks
        inner = jnp.dot(triangle, log_block, precision=high)
        spread = jnp.where(lower_cube, inner[:, None, :] - inner[None, :, :], 0.0)
        weight = jnp.where(lower_cube, jnp.exp(spread), 0.0)
        weight_real = weight * lag_cos
        weight_imag = weight * lag_sin
        new_real = jnp.sum(weight_real * real_block[None] - weight_imag * imag_block[None], axis=1)
        new_imag = jnp.sum(weight_real * imag_block[None] + weight_imag * real_block[None], axis=1)
        fade = jnp.exp(inner)
        carry_real = fade * own_cos
        carry_imag = fade * own_sin
        new_real = new_real + carry_real * state_real[None] - carry_imag * state_imag[None]
        new_imag = new_imag + carry_real * state_imag[None] + carry_imag * state_real[None]
        whole_fade = jnp.exp(run_log[None] + inner)
        whole_angle = (offset + ahead)[:, None] * turn[None, :]
        prefix_real = whole_fade * jnp.cos(whole_angle)
        prefix_imag = whole_fade * jnp.sin(whole_angle)
        following = (run_log + inner[-1], new_real[-1], new_imag[-1], offset + span)
        return (following, (new_real, new_imag, prefix_real, prefix_imag))

    zero_row = jnp.zeros((columns,), jnp.float32)
    start = (zero_row, zero_row, zero_row, jnp.zeros((), jnp.float32))
    blocks = (
        log_step.reshape(n_spans, span, columns),
        push_real.reshape(n_spans, span, columns),
        push_imag.reshape(n_spans, span, columns),
    )
    final, outputs = lax.scan(advance, start, blocks)
    outputs = tuple((item.reshape(n_rows, columns) for item in outputs))
    total_fade = jnp.exp(final[0])
    totals = (
        total_fade * jnp.cos(n_rows * turn),
        total_fade * jnp.sin(n_rows * turn),
        final[1],
        final[2],
    )
    return (outputs, totals)


def per_device(
    resid,
    mix_in,
    decay_rate,
    turn_rate,
    forget,
    input_real,
    input_imag,
    output_real,
    output_imag,
    skip_gain,
    mix_gain,
    w_out,
    ffn_gain,
    gating_matrix,
    w_up,
    w_down,
):
    high = lax.Precision.HIGHEST
    n_rows, local_width = mix_in.shape
    n_groups, n_state = decay_rate.shape
    n_chan = input_real.shape[2]
    drive = mix_in.astype(jnp.float32).reshape(n_rows, n_groups, n_chan)
    in_factor = jnp.sqrt(-jnp.expm1(2.0 * decay_rate))
    push_real = jnp.einsum(
        "gph,tgh->tgp", input_real * in_factor[:, :, None], drive, precision=high
    ).reshape(n_rows, n_groups * n_state)
    push_imag = jnp.einsum(
        "gph,tgh->tgp", input_imag * in_factor[:, :, None], drive, precision=high
    ).reshape(n_rows, n_groups * n_state)
    log_step = (decay_rate[None] + forget[:, :, None]).reshape(n_rows, n_groups * n_state)
    turn = turn_rate.reshape(n_groups * n_state)
    outputs, totals = local_states(log_step, push_real, push_imag, turn)
    inner_real, inner_imag, prefix_real, prefix_imag = outputs
    ones_row = jnp.ones((n_groups * n_state,), jnp.float32)
    zeroed_row = jnp.zeros((n_groups * n_state,), jnp.float32)
    carry_in = carried_in(totals, "sp", chain, (ones_row, zeroed_row, zeroed_row, zeroed_row))
    state_real = inner_real + prefix_real * carry_in[2][None] - prefix_imag * carry_in[3][None]
    state_imag = inner_imag + prefix_real * carry_in[3][None] + prefix_imag * carry_in[2][None]
    response = (
        jnp.einsum(
            "ghp,tgp->tgh",
            output_real,
            state_real.reshape(n_rows, n_groups, n_state),
            precision=high,
        )
        - jnp.einsum(
            "ghp,tgp->tgh",
            output_imag,
            state_imag.reshape(n_rows, n_groups, n_state),
            precision=high,
        )
        + skip_gain[None] * drive
    )
    mixer_out = jax.nn.gelu(response.reshape(n_rows, local_width)).astype(jnp.bfloat16)
    swapped = lax.all_to_all(mixer_out, "tp", split_axis=0, concat_axis=1, tiled=True)
    mixed_f = swapped.astype(jnp.float32)
    normed = (
        mixed_f * lax.rsqrt(jnp.mean(mixed_f * mixed_f, axis=1, keepdims=True) + eps) * mix_gain
    ).astype(jnp.bfloat16)
    projected = jnp.dot(normed, w_out, preferred_element_type=jnp.float32)
    resid_mid = resid.astype(jnp.float32) + projected
    ffn_in = (
        resid_mid
        * lax.rsqrt(jnp.mean(resid_mid * resid_mid, axis=1, keepdims=True) + eps)
        * ffn_gain
    ).astype(jnp.bfloat16)
    gathered = lax.all_gather(ffn_in, "tp", axis=0, tiled=True)
    gate_val = jnp.dot(
        gathered,
        lax.all_gather(gating_matrix, "sp", axis=0, tiled=True),
        preferred_element_type=jnp.float32,
    )
    up_val = jnp.dot(
        gathered, lax.all_gather(w_up, "sp", axis=0, tiled=True), preferred_element_type=jnp.float32
    )
    hidden = (jax.nn.silu(gate_val) * up_val).astype(jnp.bfloat16)
    partial_value = jnp.dot(
        hidden, lax.all_gather(w_down, "sp", axis=1, tiled=True), preferred_element_type=jnp.float32
    )
    ffn = lax.psum_scatter(
        partial_value.astype(jnp.bfloat16), "tp", scatter_dimension=0, tiled=True
    ).astype(jnp.float32)
    return (resid_mid + 0.5 * ffn).astype(jnp.bfloat16)


def solution(mesh):
    placed = (
        P(("sp", "tp"), None),
        P("sp", "tp"),
        P("tp", None),
        P("tp", None),
        P("sp", "tp"),
        P("tp", None, None),
        P("tp", None, None),
        P("tp", None, None),
        P("tp", None, None),
        P("tp", None),
        P(),
        P(),
        P(),
        P("sp", "tp"),
        P("sp", "tp"),
        P("tp", "sp"),
    )
    return jax.shard_map(
        per_device, mesh=mesh, in_specs=placed, out_specs=P(("sp", "tp"), None), check_vma=False
    )
```

profile of v0, /device:TPU:0, one launch (start us, length us, event | category | flops | bytes accessed | tf_op | source)
XLA Modules:
  0.0 576.9 jit_solution(734002597552785004)
XLA Ops:
  6.5 0.9 negate_sqrt_fusion
  7.4 0.8 add.148
  8.2 0.8 mul.301
  9.0 0.8 mul.749
  9.8 0.9 copy.51
  10.7 2.1 convolution_bitcast_fusion.2
  12.8 1.5 copy.52
  14.2 1.1 reshape_reshape.7
  15.3 1.2 convolution_bitcast_fusion.1
  16.5 1.5 copy.53
  18.0 1.1 reshape_reshape.8
  19.2 0.3 add.150
  19.5 1.1 add.151
  20.6 1.1 broadcast_add_fusion
  21.7 93.2 %while.45 = (s32[]{:T(128)}, f32[512]{0:T(512)S(1)}, f32[512]{0:T(512)S(1)}, f32[512]{0:T(512)S(1)}, f32[]{:T(128)}, /*index=5*/f32[8,32,512]{2,1,0:T(8,128)}, f...) while((s32[]{:T(128)}, f32[512]{0:T(512)S(1)}, ...), condition=%wide.wide.region_3.4_spmd.clone.clone.clone.clone, body=%wide.wide.region_0.3_spmd.clone.clone.clone.clone.sunk | while | flops 14897220 | bytes 1351775 | solution.py:78
  21.7 0.9 dynamic-slice_bitcast_fusion.4
  22.9 9.2 %add_reduce_fusion.3 = (f32[32,512]{1,0:T(8,128)S(1)}, f32[32,512]{1,0:T(8,128)S(1)}) fusion(f32[512]{0:T(512)S(1)} %get-tuple-element.853, f32[32,32]{1,0:T(8,128)S(1)} %get-tuple-element.854, f32[32,512]{1,0:T(8,128)S(1)} %get-tuple-element.788, f32[32,512]{1,0:T(8,128)S(1)} %get-tuple-element.789, ...), kind=kLoop, calls=%fused_computation.19.clone.clone.1 | loop fusion | flops 8355840 | bytes 335872 | tf_op jit(solution)/shard_map/while/body/eval_jaxpr/reduce_sum | solution.py:58
  32.1 1.2 fusion.82
  33.4 0.9 dynamic-slice_bitcast_fusion.4
  34.5 9.2 %add_reduce_fusion.3 = (f32[32,512]{1,0:T(8,128)S(1)}, f32[32,512]{1,0:T(8,128)S(1)}) fusion(f32[512]{0:T(512)S(1)} %get-tuple-element.853, f32[32,32]{1,0:T(8,128)S(1)} %get-tuple-element.854, f32[32,512]{1,0:T(8,128)S(1)} %get-tuple-element.788, f32[32,512]{1,0:T(8,128)S(1)} %get-tuple-element.789, ...), kind=kLoop, calls=%fused_computation.19.clone.clone.1 | loop fusion | flops 8355840 | bytes 335872 | tf_op jit(solution)/shard_map/while/body/eval_jaxpr/reduce_sum | solution.py:58
  43.7 1.2 fusion.82
  45.0 0.9 dynamic-slice_bitcast_fusion.4
  46.1 9.2 %add_reduce_fusion.3 = (f32[32,512]{1,0:T(8,128)S(1)}, f32[32,512]{1,0:T(8,128)S(1)}) fusion(f32[512]{0:T(512)S(1)} %get-tuple-element.853, f32[32,32]{1,0:T(8,128)S(1)} %get-tuple-element.854, f32[32,512]{1,0:T(8,128)S(1)} %get-tuple-element.788, f32[32,512]{1,0:T(8,128)S(1)} %get-tuple-element.789, ...), kind=kLoop, calls=%fused_computation.19.clone.clone.1 | loop fusion | flops 8355840 | bytes 335872 | tf_op jit(solution)/shard_map/while/body/eval_jaxpr/reduce_sum | solution.py:58
  55.4 1.2 fusion.82
  56.7 0.9 dynamic-slice_bitcast_fusion.4
  57.8 9.2 %add_reduce_fusion.3 = (f32[32,512]{1,0:T(8,128)S(1)}, f32[32,512]{1,0:T(8,128)S(1)}) fusion(f32[512]{0:T(512)S(1)} %get-tuple-element.853, f32[32,32]{1,0:T(8,128)S(1)} %get-tuple-element.854, f32[32,512]{1,0:T(8,128)S(1)} %get-tuple-element.788, f32[32,512]{1,0:T(8,128)S(1)} %get-tuple-element.789, ...), kind=kLoop, calls=%fused_computation.19.clone.clone.1 | loop fusion | flops 8355840 | bytes 335872 | tf_op jit(solution)/shard_map/while/body/eval_jaxpr/reduce_sum | solution.py:58
  67.0 1.2 fusion.82
  68.3 0.9 dynamic-slice_bitcast_fusion.4
  69.4 9.2 %add_reduce_fusion.3 = (f32[32,512]{1,0:T(8,128)S(1)}, f32[32,512]{1,0:T(8,128)S(1)}) fusion(f32[512]{0:T(512)S(1)} %get-tuple-element.853, f32[32,32]{1,0:T(8,128)S(1)} %get-tuple-element.854, f32[32,512]{1,0:T(8,128)S(1)} %get-tuple-element.788, f32[32,512]{1,0:T(8,128)S(1)} %get-tuple-element.789, ...), kind=kLoop, calls=%fused_computation.19.clone.clone.1 | loop fusion | flops 8355840 | bytes 335872 | tf_op jit(solution)/shard_map/while/body/eval_jaxpr/reduce_sum | solution.py:58
  78.7 1.3 fusion.82
  80.0 0.9 dynamic-slice_bitcast_fusion.4
  81.1 9.2 %add_reduce_fusion.3 = (f32[32,512]{1,0:T(8,128)S(1)}, f32[32,512]{1,0:T(8,128)S(1)}) fusion(f32[512]{0:T(512)S(1)} %get-tuple-element.853, f32[32,32]{1,0:T(8,128)S(1)} %get-tuple-element.854, f32[32,512]{1,0:T(8,128)S(1)} %get-tuple-element.788, f32[32,512]{1,0:T(8,128)S(1)} %get-tuple-element.789, ...), kind=kLoop, calls=%fused_computation.19.clone.clone.1 | loop fusion | flops 8355840 | bytes 335872 | tf_op jit(solution)/shard_map/while/body/eval_jaxpr/reduce_sum | solution.py:58
  90.3 1.2 fusion.82
  91.6 0.9 dynamic-slice_bitcast_fusion.4
  92.7 9.2 %add_reduce_fusion.3 = (f32[32,512]{1,0:T(8,128)S(1)}, f32[32,512]{1,0:T(8,128)S(1)}) fusion(f32[512]{0:T(512)S(1)} %get-tuple-element.853, f32[32,32]{1,0:T(8,128)S(1)} %get-tuple-element.854, f32[32,512]{1,0:T(8,128)S(1)} %get-tuple-element.788, f32[32,512]{1,0:T(8,128)S(1)} %get-tuple-element.789, ...), kind=kLoop, calls=%fused_computation.19.clone.clone.1 | loop fusion | flops 8355840 | bytes 335872 | tf_op jit(solution)/shard_map/while/body/eval_jaxpr/reduce_sum | solution.py:58
  102.0 1.2 fusion.82
  103.3 0.9 dynamic-slice_bitcast_fusion.4
  104.4 9.2 %add_reduce_fusion.3 = (f32[32,512]{1,0:T(8,128)S(1)}, f32[32,512]{1,0:T(8,128)S(1)}) fusion(f32[512]{0:T(512)S(1)} %get-tuple-element.853, f32[32,32]{1,0:T(8,128)S(1)} %get-tuple-element.854, f32[32,512]{1,0:T(8,128)S(1)} %get-tuple-element.788, f32[32,512]{1,0:T(8,128)S(1)} %get-tuple-element.789, ...), kind=kLoop, calls=%fused_computation.19.clone.clone.1 | loop fusion | flops 8355840 | bytes 335872 | tf_op jit(solution)/shard_map/while/body/eval_jaxpr/reduce_sum | solution.py:58
  113.6 1.2 fusion.82
  114.9 27.9 %all-gather.5 = f32[8,1,512]{2,1,0:T(1,128)S(1)} all-gather(f32[1,1,512]{2,1,0:T(1,128)S(1)} %bitcast.130), channel_id=3, replica_groups=mesh['sp'=8,'tp'=4] {'sp'}, dimensions={0}, use_global_device_ids=true | all-gather | bytes 18432 | tf_op jit(solution)/shard_map/all_gather | solution.py:11
  142.9 26.1 %all-gather.4 = f32[8,1,512]{2,1,0:T(1,128)S(1)} all-gather(f32[1,1,512]{2,1,0:T(1,128)S(1)} %bitcast.129), channel_id=2, replica_groups=mesh['sp'=8,'tp'=4] {'sp'}, dimensions={0}, use_global_device_ids=true | all-gather | bytes 18432 | tf_op jit(solution)/shard_map/all_gather | solution.py:11
  169.0 26.1 %all-gather.7 = f32[8,1,512]{2,1,0:T(1,128)S(1)} all-gather(f32[1,1,512]{2,1,0:T(1,128)S(1)} %bitcast.124), channel_id=5, replica_groups=mesh['sp'=8,'tp'=4] {'sp'}, dimensions={0}, use_global_device_ids=true | all-gather | bytes 18432 | tf_op jit(solution)/shard_map/all_gather | solution.py:11
  195.1 26.1 %all-gather.6 = f32[8,1,512]{2,1,0:T(1,128)S(1)} all-gather(f32[1,1,512]{2,1,0:T(1,128)S(1)} %bitcast.122), channel_id=4, replica_groups=mesh['sp'=8,'tp'=4] {'sp'}, dimensions={0}, use_global_device_ids=true | all-gather | bytes 18432 | tf_op jit(solution)/shard_map/all_gather | solution.py:11
  221.4 1.2 reshape.127
  222.6 2.2 reshape.128
  224.9 2.2 reshape.129
  227.1 2.2 reshape.130
  229.3 2.2 multiply_add_fusion.1
  231.5 1.1 fusion.35
  232.7 1.1 fusion.33
  234.1 6.7 %all_to_all.10 = bf16[4,64,128]{2,1,0:T(8,128)(2,1)S(1)} all-to-all(bf16[4,64,128]{2,1,0:T(8,128)(2,1)S(1)} %fusion.45), channel_id=1, replica_groups=mesh['sp'=8,'tp'=4] {'tp'}, dimensions={0} | all-to-all | bytes 131072 | tf_op jit(solution)/shard_map/all_to_all | solution.py:145
  241.0 0.6 multiply_reduce_fusion
  241.6 0.8 multiply_convert_fusion
  242.5 0.7 all-gather.15.cloned.1.call-update
  243.3 0.7 all-gather.17.cloned.1.call-update
  244.0 0.5 all-gather.19.cloned.1.call-update
  244.7 10.7 %all-gather.13.cloned.1.call-done = bf16[256,2048]{1,0:T(8,128)(2,1)} async-done(((bf16[64,2048]{1,0:T(8,128)(2,1)}), bf16[256,2048]{1,0:T(8,128)(2,1)}) %all-gather.13.cloned.1.call-update) | async-done | bytes 1048592 | tf_op jit(solution)/shard_map/all_gather | solution.py:157
  255.5 94.5 %all-gather.15.cloned.1.call-done = bf16[2048,1408]{1,0:T(8,128)(2,1)} async-done(((bf16[256,1408]{1,0:T(8,128)(2,1)}), bf16[2048,1408]{1,0:T(8,128)(2,1)}) %all-gather.15.cloned.1.call-update) | async-done | bytes 5767184 | tf_op jit(solution)/shard_map/all_gather | solution.py:160
  350.0 5.9 %fusion.57 = f32[256,1408]{1,0:T(8,128)} fusion(bf16[256,2048]{1,0:T(8,128)(2,1)} %all-gather.13.cloned.1.call-done, bf16[2048,1408]{1,0:T(8,128)(2,1)} %all-gather.15.cloned.1.call-done), kind=kOutput, calls=%fused_computation.104 | convolution fusion | flops 1476395008 | bytes 8257536 | tf_op jit(solution)/shard_map/dot_general | solution.py:158
  355.9 86.8 %all-gather.17.cloned.1.call-done = bf16[2048,1408]{1,0:T(8,128)(2,1)} async-done(((bf16[256,1408]{1,0:T(8,128)(2,1)}), bf16[2048,1408]{1,0:T(8,128)(2,1)}) %all-gather.17.cloned.1.call-update) | async-done | bytes 5767184 | tf_op jit(solution)/shard_map/all_gather | solution.py:164
  442.7 93.2 %all-gather.19.cloned.1.call-done = bf16[1408,2048]{1,0:T(8,128)(2,1)} async-done(((bf16[1408,256]{1,0:T(8,128)(2,1)}), bf16[1408,2048]{1,0:T(8,128)(2,1)}) %all-gather.19.cloned.1.call-update) | async-done | bytes 5767184 | tf_op jit(solution)/shard_map/all_gather | solution.py:168
  536.0 9.5 %convolution_convert_fusion = bf16[256,2048]{1,0:T(8,128)(2,1)} fusion(bf16[1408,2048]{1,0:T(8,128)(2,1)} %all-gather.19.cloned.1.call-done, bf16[256,2048]{1,0:T(8,128)(2,1)} %all-gather.13.cloned.1.call-done, bf16[2048,1408]{1,0:T(8,128)(2,1)} %all-gather.17.cloned.1.call-done, f32[256,1408]{1,0:T(8,128)} %fusion.57), kind=kOutput, calls=%fused_computation.53 | convolution fusion | flops 2955476992 | bytes 15073280 | tf_op jit(solution)/shard_map/dot_general | solution.py:167
  545.5 23.1 %reduce-scatter.2.cloned.1.call-done = bf16[64,2048]{1,0:T(8,128)(2,1)} async-done(((bf16[256,2048]{1,0:T(8,128)(2,1)}), bf16[64,2048]{1,0:T(8,128)(2,1)}) %reduce-scatter.2.cloned.1.call-update) | async-done | bytes 262160 | tf_op jit(solution)/shard_map/reduce_scatter | solution.py:170
  568.6 1.7 add_convert_fusion
  (108 shorter events, 3.3 us)
Async XLA Ops:
  6.5 234.4 %copy-start = (bf16[512,2048]{1,0:T(8,128)(2,1)S(1)}, bf16[512,2048]{1,0:T(8,128)(2,1)}, u32[]{:S(2)}) copy-start(bf16[512,2048]{1,0:T(8,128)(2,1)} %param.31) | copy-start | bytes 6291460
  6.5 8.8 %copy-start.2 = (f32[8,64,16]{1,2,0:T(8,128)S(1)}, f32[8,64,16]{1,2,0:T(8,128)}, u32[]{:S(2)}) copy-start(f32[8,64,16]{1,2,0:T(8,128)} %param.26) | copy-start | bytes 98308
  6.5 249.0 %all-gather.13.cloned.1.call-start = ((), (), s32[]{:S(2)}) async-start(), calls=%async_computation.2 | async-start | bytes 1310720 | tf_op jit(solution)/shard_map/all_gather | solution.py:157
  15.3 3.7 copy-start.6
  229.3 2.2 copy-start.3
  229.3 3.3 copy-start.4
  229.3 3.3 copy-start.7
  231.5 9.4 %copy-start.1 = (bf16[64,2048]{1,0:T(8,128)(2,1)S(1)}, bf16[64,2048]{1,0:T(8,128)(2,1)}, u32[]{:S(2)}) copy-start(bf16[64,2048]{1,0:T(8,128)(2,1)} %param.20) | copy-start | bytes 786436
  231.5 9.4 %copy-start.8 = (f32[512]{0:T(512)S(1)}, f32[512]{0:T(512)}, u32[]{:S(2)}) copy-start(f32[512]{0:T(512)} %param.30) | copy-start | bytes 6148
  233.8 7.8 %copy-start.5 = (f32[2048]{0:T(1024)S(1)}, f32[2048]{0:T(1024)}, u32[]{:S(2)}) copy-start(f32[2048]{0:T(1024)} %param.32) | copy-start | bytes 24580
  242.5 107.6 %all-gather.15.cloned.1.call-start = ((), (), s32[]{:S(2)}) async-start(), calls=%async_computation.3 | async-start | bytes 6488064 | tf_op jit(solution)/shard_map/all_gather | solution.py:160
  243.2 199.5 %all-gather.17.cloned.1.call-start = ((), (), s32[]{:S(2)}) async-start(), calls=%async_computation.4 | async-start | bytes 6488064 | tf_op jit(solution)/shard_map/all_gather | solution.py:164
  243.9 292.0 %all-gather.19.cloned.1.call-start = ((), (), s32[]{:S(2)}) async-start(), calls=%async_computation.5 | async-start | bytes 6488064 | tf_op jit(solution)/shard_map/all_gather | solution.py:168
  244.5 324.1 %reduce-scatter.2.cloned.1.call-start = ((), (), s32[]{:S(2)}) async-start(), calls=%async_computation.6 | async-start | bytes 1310720 | tf_op jit(solution)/shard_map/reduce_scatter | solution.py:170
Sparse Core Ops, SparseCore 0:
  242.6 12.8 all-gather.12
  257.7 92.3 all-gather.14
  352.2 90.4 all-gather.16
  444.6 91.2 all-gather.18
  545.6 22.9 reduce-scatter.1
where the time goes:
time: 578 us; the launch traced here: 577 us
  waiting for transfers between devices  310 us (54%)
  blocking collectives  113 us (20%)
  other arithmetic  90.7 us (16%)
  local copies, waits for them, and re-layouts  25.5 us (4%)
  matrix products  23.1 us (4%)
  between operations  13.3 us (2%)
    all_gather x4, blocking collectives, carried_in(): gathered = jax.tree.map(lambda a: lax.all_gather(a, axis), part)  106 us
    all_gather x1, waiting for transfers between devices, per_device(): lax.all_gather(gating_matrix, 'sp', axis=0, tiled=True)  94.5 us
    all_gather x1, waiting for transfers between devices, per_device(): lax.all_gather(w_down, 'sp', axis=1, tiled=True)  93.2 us
    all_gather x1, waiting for transfers between devices, per_device(): lax.all_gather(w_up, 'sp', axis=0, tiled=True)  86.8 us
    reduce_sum x8, other arithmetic, advance(): jnp.sum(weight_real * imag_block[None] + weight_imag * real_block[None],...  73.6 us
    reduce_scatter x1, waiting for transfers between devices, per_device(): lax.psum_scatter(partial_value.astype(jnp.bfloat16), 'tp', scatter_dimens...  23.1 us
  transfers between devices with their start and end apart: 5, of which 5 were waited for; matrix products, arithmetic and copies ran while one was open for 1% of the time, Pallas kernels for 0%

commit v1 on v0

--- a/solution.py
+++ b/solution.py
@@ -1,6 +1,10 @@
+import functools
+
 import jax
 import jax.numpy as jnp
 from jax import lax
+from jax.experimental import pallas as pl
+from jax.experimental.pallas import tpu as pltpu
 from jax.sharding import PartitionSpec as P
 
 eps = 1e-06
@@ -87,7 +91,7 @@
     return (outputs, totals)
 
 
-def per_device(
+def plain_device(
     resid,
     mix_in,
     decay_rate,
@@ -173,6 +177,418 @@
     return (resid_mid + 0.5 * ffn).astype(jnp.bfloat16)
 
 
+MESH = pl.DeviceIdType.MESH
+F32 = jnp.float32
+BF16 = jnp.bfloat16
+HIGH = lax.Precision.HIGHEST
+
+
+def dot_t(a, b, precision=None):
+    return lax.dot_general(
+        a, b, (((1,), (1,)), ((), ())), precision=precision, preferred_element_type=F32
+    )
+
+
+def iota(shape, dim):
+    return lax.broadcasted_iota(jnp.int32, shape, dim)
+
+
+def layer_kernel(
+    n_sp, n_tp, inner, levels, n_chan, n_state,
+    drive_ref, forget_ref, decay_ref, cos_ref, sin_ref,
+    feed_re_ref, feed_im_ref, out_re_ref, out_im_ref, skip_ref,
+    mix_gain_ref, w_out_ref, ffn_gain_ref, resid_ref, w_ref,
+    result_ref,
+    s_re, s_im, mag, p_re, p_im, tot, tots, mixed_out, swapped, mid, tokens, weights,
+    part, got1, sum1, got2, sum2, got3,
+    own_sem, wz_send, wz_recv, wy_send, wy_recv, tot_send, tot_recv, a2a_send, a2a_recv,
+    tz_send, tz_recv, tx_send, tx_recv, tc_send, tc_recv,
+    c_send, c_recv, x_send, x_recv, z_send, z_recv,
+):
+    outer = n_sp // inner
+    sp = lax.axis_index("sp")
+    tp = lax.axis_index("tp")
+    z = sp // inner
+    y = sp % inner
+    x = tp // 2
+    c = tp % 2
+    n_x = n_tp // 2
+    other_x = [((x + e) % n_x) * 2 + c for e in range(n_x)]
+    mate = x * 2 + (1 - c)
+    n_rows, width = drive_ref.shape
+    columns = decay_ref.shape[1]
+    own_rows, depth = resid_ref.shape
+    piece = weights.shape[2]
+    hid = weights.shape[1] // 3
+
+    def remote(src, dst, send, recv, to_sp, to_tp):
+        return pltpu.make_async_remote_copy(
+            src_ref=src, dst_ref=dst, send_sem=send, recv_sem=recv,
+            device_id=(to_sp, to_tp), device_id_type=MESH,
+        )
+
+    barrier = pltpu.get_barrier_semaphore()
+    for e in range(1, n_sp):
+        pl.semaphore_signal(barrier, inc=1, device_id=((sp + e) % n_sp, tp), device_id_type=MESH)
+    for e in range(1, n_tp):
+        pl.semaphore_signal(barrier, inc=1, device_id=(sp, (tp + e) % n_tp), device_id_type=MESH)
+    pl.semaphore_wait(barrier, n_sp + n_tp - 2)
+
+    started = []
+
+    def go(copy):
+        copy.start()
+        started.append(copy)
+        return copy
+
+    def w_across(d):
+        to_z = (z + d) % outer
+        return remote(
+            w_ref.at[to_z], weights.at[sp], wz_send.at[d], wz_recv.at[d], to_z * inner + y, tp
+        )
+
+    def w_inner(d, e):
+        slot = ((z + outer - d) % outer) * inner + y
+        src = w_ref.at[z] if d == 0 else weights.at[slot]
+        return remote(
+            src, weights.at[slot], wy_send.at[d, e], wy_recv.at[d, e],
+            z * inner + (y + e) % inner, tp,
+        )
+
+    near = [1] + ([outer - 1] if outer > 2 else [])
+    far = [d for d in range(1, outer) if d not in near]
+    for e in range(1, inner):
+        go(w_inner(0, e))
+    crossing = {d: go(w_across(d)) for d in near}
+    own = pltpu.make_async_copy(w_ref.at[z], weights.at[sp], own_sem)
+    own.start()
+
+    def spread(a, groups):
+        low = a.shape[1]
+        pick = (iota((low, low * groups), 1) % low == iota((low, low * groups), 0)).astype(F32)
+        return jnp.dot(a, pick, precision=HIGH, preferred_element_type=F32)
+
+    n_groups = width // n_chan
+    drive = drive_ref[...].astype(F32)
+    to_state = iota((columns, width), 0) // n_state == iota((columns, width), 1) // n_chan
+    s_re[...] = dot_t(drive, jnp.where(to_state, spread(feed_re_ref[...], n_groups), 0.0), HIGH)
+    s_im[...] = dot_t(drive, jnp.where(to_state, spread(feed_im_ref[...], n_groups), 0.0), HIGH)
+    group_of = (iota((n_groups, columns), 1) // n_state == iota((n_groups, columns), 0)).astype(F32)
+    mag[...] = jnp.exp(
+        decay_ref[...]
+        + jnp.dot(forget_ref[...], group_of, precision=HIGH, preferred_element_type=F32)
+    )
+
+    def scan_block(i, carry):
+        cols = pl.ds(pl.multiple_of(i * 128, 128), 128)
+        row = iota((n_rows, 128), 0)
+        a, re, im = mag[:, cols], s_re[:, cols], s_im[:, cols]
+        for k in range(levels):
+            shift = 2**k
+            inside = row >= shift
+            w = jnp.where(inside, a, 0.0)
+            w_re = w * cos_ref[k : k + 1, cols]
+            w_im = w * sin_ref[k : k + 1, cols]
+            b_re = pltpu.roll(re, shift, 0)
+            b_im = pltpu.roll(im, shift, 0)
+            re = re + w_re * b_re - w_im * b_im
+            im = im + w_re * b_im + w_im * b_re
+            a = a * jnp.where(inside, pltpu.roll(a, shift, 0), 1.0)
+        mag[:, cols] = a
+        s_re[:, cols] = re
+        s_im[:, cols] = im
+        return carry
+
+    lax.fori_loop(0, columns // 128, scan_block, 0)
+    last = n_rows - 1
+    tot[0:1, :] = mag[last : last + 1, :]
+    tot[1:2, :] = s_re[last : last + 1, :]
+    tot[2:3, :] = s_im[last : last + 1, :]
+    tot[3:8, :] = jnp.zeros((5, columns), F32)
+    tots[sp] = tot[...]
+    totals = [
+        go(remote(tot, tots.at[sp], tot_send.at[e], tot_recv.at[e], (sp + e) % n_sp, tp))
+        for e in range(1, n_sp)
+    ]
+    for d in far:
+        crossing[d] = go(w_across(d))
+
+    def prefix_block(i, carry):
+        cols = pl.ds(pl.multiple_of(i * 128, 128), 128)
+        row = iota((n_rows, 128), 0)
+        r_re = jnp.zeros((n_rows, 128), F32) + cos_ref[0:1, cols]
+        r_im = jnp.zeros((n_rows, 128), F32) + sin_ref[0:1, cols]
+        for k in range(levels):
+            bit = (row // 2**k) % 2 == 1
+            m_re = jnp.where(bit, cos_ref[k : k + 1, cols], 1.0)
+            m_im = jnp.where(bit, sin_ref[k : k + 1, cols], 0.0)
+            r_re, r_im = r_re * m_re - r_im * m_im, r_re * m_im + r_im * m_re
+        p_re[:, cols] = mag[:, cols] * r_re
+        p_im[:, cols] = mag[:, cols] * r_im
+        return carry
+
+    lax.fori_loop(0, columns // 128, prefix_block, 0)
+    to_chan_re = jnp.where(
+        iota((width, columns), 1) // n_state == iota((width, columns), 0) // n_chan,
+        spread(out_re_ref[...], n_groups), 0.0)
+    to_chan_im = jnp.where(
+        iota((width, columns), 1) // n_state == iota((width, columns), 0) // n_chan,
+        spread(out_im_ref[...], n_groups), 0.0)
+    for copy in totals:
+        copy.wait_recv()
+    in_re = jnp.zeros((1, columns), F32)
+    in_im = jnp.zeros((1, columns), F32)
+    full_cos = cos_ref[levels : levels + 1, :]
+    full_sin = sin_ref[levels : levels + 1, :]
+    for j in range(n_sp):
+        there = tots[j]
+        t_re = there[0:1] * full_cos
+        t_im = there[0:1] * full_sin
+        n_re = t_re * in_re - t_im * in_im + there[1:2]
+        n_im = t_re * in_im + t_im * in_re + there[2:3]
+        earlier = j < sp
+        in_re = jnp.where(earlier, n_re, in_re)
+        in_im = jnp.where(earlier, n_im, in_im)
+    state_re = s_re[...] + p_re[...] * in_re - p_im[...] * in_im
+    state_im = s_im[...] + p_re[...] * in_im + p_im[...] * in_re
+    response = (
+        dot_t(state_re, to_chan_re, HIGH) - dot_t(state_im, to_chan_im, HIGH)
+        + skip_ref[...] * drive
+    )
+    mixed_out[...] = jax.nn.gelu(response).astype(BF16).reshape(n_tp, own_rows, width)
+    swaps = []
+    for e in range(1, n_tp):
+        to = (tp + e) % n_tp
+        swaps.append(
+            go(remote(mixed_out.at[to], swapped.at[tp], a2a_send.at[e], a2a_recv.at[e], sp, to))
+        )
+    swapped[tp] = mixed_out[tp]
+    inward = []
+    for d in near:
+        crossing[d].wait_recv()
+        for e in range(1, inner):
+            inward.append(go(w_inner(d, e)))
+    for copy in swaps:
+        copy.wait_recv()
+    mixed_f = jnp.concatenate([swapped[j] for j in range(n_tp)], axis=1).astype(F32)
+    normed = (
+        mixed_f
+        * lax.rsqrt(jnp.mean(mixed_f * mixed_f, axis=1, keepdims=True) + eps)
+        * mix_gain_ref[...]
+    ).astype(BF16)
+    resid_mid = resid_ref[...].astype(F32) + jnp.dot(
+        normed, w_out_ref[...], preferred_element_type=F32
+    )
+    mid[...] = resid_mid
+    home = z * n_tp + tp
+    tokens[home] = (
+        resid_mid
+        * lax.rsqrt(jnp.mean(resid_mid * resid_mid, axis=1, keepdims=True) + eps)
+        * ffn_gain_ref[...]
+    ).astype(BF16)
+
+    def slot_of(d, who):
+        return ((z + outer - d) % outer) * n_tp + who
+
+    def to_x(d, e):
+        s = slot_of(d, tp)
+        return remote(
+            tokens.at[s], tokens.at[s], tx_send.at[d, e], tx_recv.at[d, e], sp, other_x[e]
+        )
+
+    def to_mate(d, e):
+        s = slot_of(d, other_x[(n_x - e) % n_x])
+        return remote(tokens.at[s], tokens.at[s], tc_send.at[d, e], tc_recv.at[d, e], sp, mate)
+
+    t_across = {}
+    order = near + far
+    for d in order:
+        t_across[d] = go(
+            remote(
+                tokens.at[home], tokens.at[home], tz_send.at[d], tz_recv.at[d],
+                ((z + d) % outer) * inner + y, tp,
+            )
+        )
+    arrive_x, arrive_mate = {}, []
+    for d in [0] + order:
+        if d:
+            t_across[d].wait_recv()
+        for e in range(1, n_x):
+            arrive_x[d, e] = go(to_x(d, e))
+        arrive_mate.append(go(to_mate(d, 0)))
+    for d in far:
+        crossing[d].wait_recv()
+        for e in range(1, inner):
+            inward.append(go(w_inner(d, e)))
+    for d in [0] + order:
+        for e in range(1, n_x):
+            arrive_x[d, e].wait_recv()
+            arrive_mate.append(go(to_mate(d, e)))
+    for copy in arrive_mate:
+        copy.wait_recv()
+    own.wait()
+    for e in range(1, inner):
+        w_inner(0, e).wait_recv()
+    for copy in inward:
+        copy.wait_recv()
+
+    def step1(i, k):
+        return remote(
+            part.at[i, k * 2 + (1 - c)], got1.at[i, k], c_send.at[i, k], c_recv.at[i, k], sp, mate
+        )
+
+    def step2(i, e):
+        to = (x + e) % n_x
+        return remote(
+            sum1.at[i, to], got2.at[i, e], x_send.at[i, e], x_recv.at[i, e], sp, to * 2 + c
+        )
+
+    def step3(i):
+        to_z = (z + i + 1) % outer
+        return remote(
+            sum2.at[i], got3.at[i], z_send.at[i], z_recv.at[i], to_z * inner + y, tp
+        )
+
+    def flow(i, carry):
+        @pl.when(i < outer)
+        def _():
+            to_z = (z + i + 1) % outer
+            block = tokens[pl.ds(to_z * n_tp, n_tp)].reshape(n_tp * own_rows, depth)
+            both = jnp.zeros((n_tp * own_rows, 2 * hid), F32)
+            for k in range(n_sp):
+                both += dot_t(block[:, k * piece : (k + 1) * piece], weights[k, 0 : 2 * hid, :])
+            hidden = (jax.nn.silu(both[:, :hid]) * both[:, hid:]).astype(BF16)
+            for k in range(n_sp):
+                value = jnp.dot(hidden, weights[k, 2 * hid :, :], preferred_element_type=F32)
+                part[i, :, :, k * piece : (k + 1) * piece] = value.astype(BF16).reshape(
+                    n_tp, own_rows, piece
+                )
+            for k in range(n_x):
+                step1(i, k).start()
+
+        @pl.when((i >= 1) & (i < outer + 1))
+        def _():
+            for k in range(n_x):
+                step1(i - 1, k).wait()
+                sum1[i - 1, k] = (
+                    part[i - 1, k * 2 + c].astype(F32) + got1[i - 1, k].astype(F32)
+                ).astype(BF16)
+            for e in range(1, n_x):
+                step2(i - 1, e).start()
+
+        @pl.when((i >= 2) & (i < outer + 2))
+        def _():
+            total = sum1[i - 2, x].astype(F32)
+            for e in range(1, n_x):
+                step2(i - 2, e).wait()
+                total += got2[i - 2, e].astype(F32)
+            sum2[i - 2] = total.astype(BF16)
+
+            @pl.when(i - 2 < outer - 1)
+            def _():
+                step3(i - 2).start()
+
+        return carry
+
+    lax.fori_loop(0, outer + 2, flow, 0)
+    ffn = sum2[outer - 1].astype(F32)
+    for i in range(outer - 1):
+        step3(i).wait()
+        ffn += got3[i].astype(F32)
+    result_ref[...] = (mid[...] + 0.5 * ffn).astype(BF16)
+    for copy in started:
+        copy.wait_send()
+
+
+def fused_device(
+    n_sp, n_tp, inner,
+    resid, mix_in, decay_rate, turn_rate, forget, input_real, input_imag, output_real,
+    output_imag, skip_gain, mix_gain, w_out, ffn_gain, gating_matrix, w_up, w_down,
+):
+    outer = n_sp // inner
+    n_rows, width = mix_in.shape
+    n_groups, n_state = decay_rate.shape
+    n_chan = input_real.shape[2]
+    columns = n_groups * n_state
+    levels = n_rows.bit_length() - 1
+    own_rows, depth = resid.shape
+    piece, n_hid = gating_matrix.shape
+    hid = n_hid // outer
+    in_factor = jnp.sqrt(-jnp.expm1(2.0 * decay_rate))[:, :, None]
+    feed_re = (input_real * in_factor).reshape(columns, n_chan)
+    feed_im = (input_imag * in_factor).reshape(columns, n_chan)
+    powers = 2.0 ** jnp.arange(levels + 1, dtype=F32)
+    angle = powers[:, None] * turn_rate.reshape(1, columns)
+    w = jnp.concatenate(
+        [
+            gating_matrix.T.reshape(outer, hid, piece),
+            w_up.T.reshape(outer, hid, piece),
+            w_down.reshape(outer, hid, piece),
+        ],
+        axis=1,
+    )
+    vmem = pl.BlockSpec(memory_space=pltpu.VMEM)
+    n_x = n_tp // 2
+    dma = pltpu.SemaphoreType.DMA
+    wide = pltpu.VMEM((n_rows, columns), F32)
+    block = (own_rows, depth)
+    return pl.pallas_call(
+        functools.partial(layer_kernel, n_sp, n_tp, inner, levels, n_chan, n_state),
+        out_shape=jax.ShapeDtypeStruct(resid.shape, BF16),
+        in_specs=[vmem] * 14 + [pl.BlockSpec(memory_space=pl.ANY)],
+        out_specs=vmem,
+        scratch_shapes=[
+            wide, wide, wide, wide, wide,
+            pltpu.VMEM((8, columns), F32),
+            pltpu.VMEM((n_sp, 8, columns), F32),
+            pltpu.VMEM((n_tp, own_rows, width), BF16),
+            pltpu.VMEM((n_tp, own_rows, width), BF16),
+            pltpu.VMEM(block, F32),
+            pltpu.VMEM((outer * n_tp,) + block, BF16),
+            pltpu.VMEM((n_sp, 3 * hid, piece), BF16),
+            pltpu.VMEM((outer, n_tp) + block, BF16),
+            pltpu.VMEM((outer, n_x) + block, BF16),
+            pltpu.VMEM((outer, n_x) + block, BF16),
+            pltpu.VMEM((outer, n_x) + block, BF16),
+            pltpu.VMEM((outer,) + block, BF16),
+            pltpu.VMEM((outer,) + block, BF16),
+            dma, dma((outer,)), dma((outer,)), dma((outer, inner)), dma((outer, inner)),
+            dma((n_sp,)), dma((n_sp,)), dma((n_tp,)), dma((n_tp,)),
+            dma((outer,)), dma((outer,)), dma((outer, n_x)), dma((outer, n_x)),
+            dma((outer, n_x)), dma((outer, n_x)),
+            dma((outer, n_x)), dma((outer, n_x)), dma((outer, n_x)), dma((outer, n_x)),
+            dma((outer,)), dma((outer,)),
+        ],
+        compiler_params=pltpu.CompilerParams(
+            collective_id=0, has_side_effects=True, vmem_limit_bytes=60 * 2**20
+        ),
+        name="layer",
+    )(
+        mix_in, forget, decay_rate.reshape(1, columns), jnp.cos(angle), jnp.sin(angle),
+        feed_re, feed_im,
+        output_real.reshape(width, n_state), output_imag.reshape(width, n_state),
+        skip_gain.reshape(1, width), mix_gain.reshape(1, -1), w_out, ffn_gain.reshape(1, -1),
+        resid, w,
+    )
+
+
+def per_device(n_sp, n_tp, *args):
+    mix_in, gating_matrix = args[1], args[13]
+    inner = 2
+    n_rows, width = mix_in.shape
+    columns = args[2].shape[0] * args[2].shape[1]
+    piece, n_hid = gating_matrix.shape
+    fits = (
+        n_sp % inner == 0 and n_sp <= 8 and n_tp % 2 == 0
+        and n_hid % (16 * (n_sp // inner)) == 0
+        and piece % 128 == 0 and width % 128 == 0 and columns % 128 == 0
+        and n_rows & (n_rows - 1) == 0
+    )
+    if fits:
+        return fused_device(n_sp, n_tp, inner, *args)
+    return plain_device(*args)
+
+
 def solution(mesh):
     placed = (
         P(("sp", "tp"), None),
@@ -193,5 +609,5 @@
         P("tp", "sp"),
     )
     return jax.shard_map(
-        per_device, mesh=mesh, in_specs=placed, out_specs=P(("sp", "tp"), None), check_vma=False
-    )
+        functools.partial(per_device, mesh.shape["sp"], mesh.shape["tp"]), mesh=mesh, in_specs=placed, out_specs=P(("sp", "tp"), None), check_vma=False
+    )

time: 578 us -> 142 us (0.25)
  waiting for transfers between devices: 310 us -> 0 us
  Pallas kernels: 0 us -> 127 us
  blocking collectives: 113 us -> 0 us
  other arithmetic: 90.7 us -> 4.02 us
  matrix products: 23.1 us -> 0 us
  local copies, waits for them, and re-layouts: 25.5 us -> 7.89 us
  between operations: 13.3 us -> 0.07 us
    all_gather x4 -> x0, waiting for transfers between devices: 285 us -> none  [the longest x1 94.5 us: per_device(): lax.all_gather(gating_matrix, 'sp', axis=0, tiled=True)]
    pallas_call x0 -> x1, Pallas kernels: none -> 127 us  [fused_device(): pl.pallas_call(functools.partial(layer_kernel, n_sp, n_tp, inner, levels,...]
    all_gather x4 -> x0, blocking collectives: 106 us -> none  [carried_in(): gathered = jax.tree.map(lambda a: lax.all_gather(a, axis), part)]
    reduce_sum x9 -> x0, other arithmetic: 73.7 us -> none  [the longest x8 73.6 us: advance(): jnp.sum(weight_real * imag_block[None] + weight_imag * real_block[None],...]
    dot_general x15 -> x0, matrix products: 23.1 us -> none  [the longest x1 9.51 us: per_device(): jnp.dot(hidden, lax.all_gather(w_down, 'sp', axis=1, tiled=True), preferr...]
    reduce_scatter x1 -> x0, waiting for transfers between devices: 23.1 us -> none  [per_device(): lax.psum_scatter(partial_value.astype(jnp.bfloat16), 'tp', scatter_dimens...]
    dynamic_update_slice x8 -> x0, other arithmetic: 9.93 us -> none  [local_states(): final, outputs = lax.scan(advance, start, blocks)]
    reshape x6 -> x2, local copies, waits for them, and re-layouts: 8.21 us -> 1.31 us  [the longest x1 0.66 us: fused_device(): decay_rate.reshape(1, columns)]
  transfers between devices with their start and end apart: 5 -> 0, of which waited for: 5 -> 0; matrix products, arithmetic and copies ran while one was open for 1% -> 0% of each run, Pallas kernels for 0% -> 0%
where the time goes in v1:
time: 142 us; the launch traced here: 139 us
  Pallas kernels  127 us (89%)
  local copies, waits for them, and re-layouts  7.89 us (6%)
  other arithmetic  4.02 us (3%)
    pallas_call x1, Pallas kernels, fused_device(): pl.pallas_call(functools.partial(layer_kernel, n_sp, n_tp, inner, levels,...  127 us

profile of v1, /device:TPU:0, one launch (start us, length us, event | category | flops | bytes accessed | tf_op | source)
XLA Modules:
  0.0 139.1 jit_solution(9949932594921086532)
XLA Ops:
  0.0 0.0 copy-start
  0.0 0.0 copy-start.1
  0.0 0.8 negate_sqrt_fusion
  0.8 0.9 broadcast_multiply_fusion
  1.7 0.8 copy.17
  2.5 0.8 copy.18
  3.4 0.8 mul.36
  4.1 0.8 multiply_sine_fusion
  5.0 1.4 copy.19
  6.4 0.0 copy-done
  6.4 0.3 copy.20
  6.7 0.0 copy-done.1
  6.7 0.0 copy-start.3
  6.7 0.0 copy-start.2
  6.7 0.0 copy-start.4
  6.7 1.5 %pad_maximum_fusion.w_ref = bf16[4,1056,256]{2,1,0:T(8,128)(2,1)} fusion(bf16[4,352,256]{2,1,0:T(8,128)(2,1)S(1)} %bitcast.17, bf16[4,352,256]{2,1,0:T(8,128)(2,1)S(1)} %bitcast.12, bf16[4,352,256]{2,1,0:T(8,128)(2,1)S(1)} %bitcast.11), kind=kLoop, calls=%fused_computation | loop fusion | flops 6488064 | bytes 4325376 | tf_op jit(solution)/shard_map/concatenate | solution.py:522
  8.2 0.0 copy-done.3
  8.2 0.8 copy.21.forget_ref
  9.0 0.0 copy-done.2
  9.0 0.7 reshape.40.decay_ref
  9.6 0.0 copy-done.4
  9.7 0.6 reshape.45.skip_ref
  10.3 127.2 %layer.1 = bf16[64,2048]{1,0:T(8,128)(2,1)} custom-call(bf16[256,128]{1,0:T(8,128)(2,1)} %drive_ref.1, f32[256,8]{1,0:T(8,128)} %copy.21.forget_ref, f32[1,512]{1,0:T(1,128)} %reshape.40.decay_ref, f32[9,512]{1,0:T(8,128)} %get-tuple-element.8.cos_ref, f32[9,512]{1,0:T(8,128)} %get-tuple-element.7.sin_ref, f32[512,16]{1,0:T(8,128)} %bitcast.13, ...), custom_call_target="tpu_custom_call" | custom-call | tf_op jit(solution)/shard_map/layer/pallas_call | solution.py:535
  137.5 1.7 %copy.23 = bf16[64,2048]{1,0:T(8,128)(2,1)} copy(bf16[64,2048]{1,0:T(8,128)(2,1)} %layer.1) | data formatting | bytes 524288
  (1 shorter events, 0.0 us)
Async XLA Ops:
  0.0 6.4 %copy-start = (bf16[256,1408]{1,0:T(8,128)(2,1)S(1)}, bf16[256,1408]{1,0:T(8,128)(2,1)}, u32[]{:S(2)}) copy-start(bf16[256,1408]{1,0:T(8,128)(2,1)} %param.30) | copy-start | bytes 2162692
  0.0 6.7 %copy-start.1 = (bf16[1408,256]{1,0:T(8,128)(2,1)S(1)}, bf16[1408,256]{1,0:T(8,128)(2,1)}, u32[]{:S(2)}) copy-start(bf16[1408,256]{1,0:T(8,128)(2,1)} %param.31) | copy-start | bytes 2162692
  6.7 1.5 %copy-start.3 = (f32[256,8]{0,1:T(8,128)S(1)}, f32[256,8]{0,1:T(8,128)}, u32[]{:S(2)}) copy-start(f32[256,8]{0,1:T(8,128)} %param.20) | copy-start | bytes 24580
  6.7 2.3 %copy-start.2 = (f32[8,64]{1,0:T(8,128)S(1)}, f32[8,64]{1,0:T(8,128)}, u32[]{:S(2)}) copy-start(f32[8,64]{1,0:T(8,128)} %param.18) | copy-start | bytes 6148
  6.7 3.0 %copy-start.4 = (f32[8,16]{1,0:T(8,128)S(1)}, f32[8,16]{1,0:T(8,128)}, u32[]{:S(2)}) copy-start(f32[8,16]{1,0:T(8,128)} %param.25) | copy-start | bytes 1540

commit v2 on v1

--- a/solution.py
+++ b/solution.py
@@ -193,13 +193,20 @@
     return lax.broadcasted_iota(jnp.int32, shape, dim)
 
 
+def one_minus_exp(a):
+    series = jnp.ones_like(a)
+    for k in range(10, 1, -1):
+        series = 1.0 + series * a * (1.0 / k)
+    return jnp.where(a > -0.3, -a * series, 1.0 - jnp.exp(a))
+
+
 def layer_kernel(
     n_sp, n_tp, inner, levels, n_chan, n_state,
-    drive_ref, forget_ref, decay_ref, cos_ref, sin_ref,
+    drive_ref, forget_ref, decay_ref, turn_ref,
     feed_re_ref, feed_im_ref, out_re_ref, out_im_ref, skip_ref,
     mix_gain_ref, w_out_ref, ffn_gain_ref, resid_ref, w_ref,
     result_ref,
-    s_re, s_im, mag, p_re, p_im, tot, tots, mixed_out, swapped, mid, tokens, weights,
+    cos_ref, sin_ref, s_re, s_im, mag, p_re, p_im, tot, tots, mixed_out, swapped, mid, tokens, weights,
     part, got1, sum1, got2, sum2, got3,
     own_sem, wz_send, wz_recv, wy_send, wy_recv, tot_send, tot_recv, a2a_send, a2a_recv,
     tz_send, tz_recv, tx_send, tx_recv, tc_send, tc_recv,
@@ -216,7 +223,7 @@
     other_x = [((x + e) % n_x) * 2 + c for e in range(n_x)]
     mate = x * 2 + (1 - c)
     n_rows, width = drive_ref.shape
-    columns = decay_ref.shape[1]
+    columns = decay_ref.shape[0] * n_state
     own_rows, depth = resid_ref.shape
     piece = weights.shape[2]
     hid = weights.shape[1] // 3
@@ -241,14 +248,20 @@
         started.append(copy)
         return copy
 
+    def across(d):
+        there = z
+        for k in range(outer.bit_length() - 1):
+            there += ((d // 2**k) % 2) * (2**k - 2 ** (k + 1) * ((z // 2**k) % 2))
+        return there
+
     def w_across(d):
-        to_z = (z + d) % outer
+        to_z = across(d)
         return remote(
             w_ref.at[to_z], weights.at[sp], wz_send.at[d], wz_recv.at[d], to_z * inner + y, tp
         )
 
     def w_inner(d, e):
-        slot = ((z + outer - d) % outer) * inner + y
+        slot = across(d) * inner + y
         src = w_ref.at[z] if d == 0 else weights.at[slot]
         return remote(
             src, weights.at[slot], wy_send.at[d, e], wy_recv.at[d, e],
@@ -257,6 +270,7 @@
 
     near = [1] + ([outer - 1] if outer > 2 else [])
     far = [d for d in range(1, outer) if d not in near]
+    first, rest = near[:1], near[1:]
     for e in range(1, inner):
         go(w_inner(0, e))
     crossing = {d: go(w_across(d)) for d in near}
@@ -270,13 +284,39 @@
 
     n_groups = width // n_chan
     drive = drive_ref[...].astype(F32)
-    to_state = iota((columns, width), 0) // n_state == iota((columns, width), 1) // n_chan
-    s_re[...] = dot_t(drive, jnp.where(to_state, spread(feed_re_ref[...], n_groups), 0.0), HIGH)
-    s_im[...] = dot_t(drive, jnp.where(to_state, spread(feed_im_ref[...], n_groups), 0.0), HIGH)
-    group_of = (iota((n_groups, columns), 1) // n_state == iota((n_groups, columns), 0)).astype(F32)
+    group_of = iota((n_groups, columns), 1) // n_state == iota((n_groups, columns), 0)
+
+    def as_row(a, per):
+        groups, wide = a.shape[0], a.shape[0] * per
+        mine = iota((groups, wide), 1) // per == iota((groups, wide), 0)
+        return jnp.sum(jnp.where(mine, spread(a, groups), 0.0), axis=0, keepdims=True)
+
+    decay = as_row(decay_ref[...], n_state)
+    turn = as_row(turn_ref[...], n_state)
+    rows = cos_ref.shape[0]
+    power = jnp.zeros((rows, columns), F32)
+    for k in range(levels + 1):
+        power = jnp.where(iota((rows, columns), 0) == k, float(2**k), power)
+    cos_ref[...] = jnp.cos(power * turn)
+    sin_ref[...] = jnp.sin(power * turn)
+    in_factor = jnp.sqrt(one_minus_exp(2.0 * decay))
+    matching = iota((width, columns), 1) // n_state == iota((width, columns), 0) // n_chan
+
+    def expanded(ref):
+        return jnp.where(matching, spread(ref[...], n_groups), 0.0)
+
+    s_re[...] = in_factor * jnp.dot(
+        drive, expanded(feed_re_ref), precision=HIGH, preferred_element_type=F32
+    )
+    s_im[...] = in_factor * jnp.dot(
+        drive, expanded(feed_im_ref), precision=HIGH, preferred_element_type=F32
+    )
     mag[...] = jnp.exp(
-        decay_ref[...]
-        + jnp.dot(forget_ref[...], group_of, precision=HIGH, preferred_element_type=F32)
+        decay
+        + lax.dot_general(
+            forget_ref[...], group_of.astype(F32), (((0,), (0,)), ((), ())),
+            precision=HIGH, preferred_element_type=F32,
+        )
     )
 
     def scan_block(i, carry):
@@ -313,6 +353,12 @@
     for d in far:
         crossing[d] = go(w_across(d))
 
+    inward = []
+    for d in first:
+        crossing[d].wait_recv()
+        for e in range(1, inner):
+            inward.append(go(w_inner(d, e)))
+
     def prefix_block(i, carry):
         cols = pl.ds(pl.multiple_of(i * 128, 128), 128)
         row = iota((n_rows, 128), 0)
@@ -328,12 +374,9 @@
         return carry
 
     lax.fori_loop(0, columns // 128, prefix_block, 0)
-    to_chan_re = jnp.where(
-        iota((width, columns), 1) // n_state == iota((width, columns), 0) // n_chan,
-        spread(out_re_ref[...], n_groups), 0.0)
-    to_chan_im = jnp.where(
-        iota((width, columns), 1) // n_state == iota((width, columns), 0) // n_chan,
-        spread(out_im_ref[...], n_groups), 0.0)
+    to_chan_re = expanded(out_re_ref)
+    to_chan_im = expanded(out_im_ref)
+    skip_row = as_row(skip_ref[...], n_chan)
     for copy in totals:
         copy.wait_recv()
     in_re = jnp.zeros((1, columns), F32)
@@ -353,7 +396,7 @@
     state_im = s_im[...] + p_re[...] * in_im + p_im[...] * in_re
     response = (
         dot_t(state_re, to_chan_re, HIGH) - dot_t(state_im, to_chan_im, HIGH)
-        + skip_ref[...] * drive
+        + skip_row * drive
     )
     mixed_out[...] = jax.nn.gelu(response).astype(BF16).reshape(n_tp, own_rows, width)
     swaps = []
@@ -363,8 +406,7 @@
             go(remote(mixed_out.at[to], swapped.at[tp], a2a_send.at[e], a2a_recv.at[e], sp, to))
         )
     swapped[tp] = mixed_out[tp]
-    inward = []
-    for d in near:
+    for d in rest:
         crossing[d].wait_recv()
         for e in range(1, inner):
             inward.append(go(w_inner(d, e)))
@@ -388,7 +430,7 @@
     ).astype(BF16)
 
     def slot_of(d, who):
-        return ((z + outer - d) % outer) * n_tp + who
+        return across(d) * n_tp + who
 
     def to_x(d, e):
         s = slot_of(d, tp)
@@ -406,9 +448,13 @@
         t_across[d] = go(
             remote(
                 tokens.at[home], tokens.at[home], tz_send.at[d], tz_recv.at[d],
-                ((z + d) % outer) * inner + y, tp,
+                across(d) * inner + y, tp,
             )
         )
+    for d in far:
+        crossing[d].wait_recv()
+        for e in range(1, inner):
+            inward.append(go(w_inner(d, e)))
     arrive_x, arrive_mate = {}, []
     for d in [0] + order:
         if d:
@@ -416,10 +462,6 @@
         for e in range(1, n_x):
             arrive_x[d, e] = go(to_x(d, e))
         arrive_mate.append(go(to_mate(d, 0)))
-    for d in far:
-        crossing[d].wait_recv()
-        for e in range(1, inner):
-            inward.append(go(w_inner(d, e)))
     for d in [0] + order:
         for e in range(1, n_x):
             arrive_x[d, e].wait_recv()
@@ -444,7 +486,7 @@
         )
 
     def step3(i):
-        to_z = (z + i + 1) % outer
+        to_z = across(outer - 1 - i)
         return remote(
             sum2.at[i], got3.at[i], z_send.at[i], z_recv.at[i], to_z * inner + y, tp
         )
@@ -452,7 +494,7 @@
     def flow(i, carry):
         @pl.when(i < outer)
         def _():
-            to_z = (z + i + 1) % outer
+            to_z = across(outer - 1 - i)
             block = tokens[pl.ds(to_z * n_tp, n_tp)].reshape(n_tp * own_rows, depth)
             both = jnp.zeros((n_tp * own_rows, 2 * hid), F32)
             for k in range(n_sp):
@@ -514,11 +556,8 @@
     own_rows, depth = resid.shape
     piece, n_hid = gating_matrix.shape
     hid = n_hid // outer
-    in_factor = jnp.sqrt(-jnp.expm1(2.0 * decay_rate))[:, :, None]
-    feed_re = (input_real * in_factor).reshape(columns, n_chan)
-    feed_im = (input_imag * in_factor).reshape(columns, n_chan)
-    powers = 2.0 ** jnp.arange(levels + 1, dtype=F32)
-    angle = powers[:, None] * turn_rate.reshape(1, columns)
+    feed_re = jnp.swapaxes(input_real, 1, 2).reshape(width, n_state)
+    feed_im = jnp.swapaxes(input_imag, 1, 2).reshape(width, n_state)
     w = jnp.concatenate(
         [
             gating_matrix.T.reshape(outer, hid, piece),
@@ -535,9 +574,10 @@
     return pl.pallas_call(
         functools.partial(layer_kernel, n_sp, n_tp, inner, levels, n_chan, n_state),
         out_shape=jax.ShapeDtypeStruct(resid.shape, BF16),
-        in_specs=[vmem] * 14 + [pl.BlockSpec(memory_space=pl.ANY)],
+        in_specs=[vmem] * 13 + [pl.BlockSpec(memory_space=pl.ANY)],
         out_specs=vmem,
         scratch_shapes=[
+            pltpu.VMEM((16, columns), F32), pltpu.VMEM((16, columns), F32),
             wide, wide, wide, wide, wide,
             pltpu.VMEM((8, columns), F32),
             pltpu.VMEM((n_sp, 8, columns), F32),
@@ -564,10 +604,10 @@
         ),
         name="layer",
     )(
-        mix_in, forget, decay_rate.reshape(1, columns), jnp.cos(angle), jnp.sin(angle),
+        mix_in, forget.T, decay_rate, turn_rate,
         feed_re, feed_im,
         output_real.reshape(width, n_state), output_imag.reshape(width, n_state),
-        skip_gain.reshape(1, width), mix_gain.reshape(1, -1), w_out, ffn_gain.reshape(1, -1),
+        skip_gain, mix_gain.reshape(1, -1), w_out, ffn_gain.reshape(1, -1),
         resid, w,
     )
 
@@ -579,10 +619,10 @@
     columns = args[2].shape[0] * args[2].shape[1]
     piece, n_hid = gating_matrix.shape
     fits = (
-        n_sp % inner == 0 and n_sp <= 8 and n_tp % 2 == 0
+        n_sp in (2 * inner, 4 * inner) and n_tp % 2 == 0
         and n_hid % (16 * (n_sp // inner)) == 0
         and piece % 128 == 0 and width % 128 == 0 and columns % 128 == 0
-        and n_rows & (n_rows - 1) == 0
+        and n_rows & (n_rows - 1) == 0 and n_rows < 2**15
     )
     if fits:
         return fused_device(n_sp, n_tp, inner, *args)

time: 142 us -> 134 us (0.944); the launches traced: 139 us -> 134 us
  local copies, waits for them, and re-layouts: 7.89 us -> 4.5 us
  other arithmetic: 4.02 us -> 1.49 us
    mul x3 -> x0, local copies, waits for them, and re-layouts: 2.43 us -> none  [the longest x1 0.84 us: fused_device(): feed_re = (input_real * in_factor).reshape(columns, n_chan)]
where the time goes in v2:
time: 134 us
  Pallas kernels  128 us (96%)
  local copies, waits for them, and re-layouts  4.5 us (3%)
  other arithmetic  1.49 us (1%)
    pallas_call x1, Pallas kernels, fused_device(): pl.pallas_call(functools.partial(layer_kernel, n_sp, n_tp, inner, levels,...  128 us

profile of v2, /device:TPU:0, one launch (start us, length us, event | category | flops | bytes accessed | tf_op | source)
XLA Modules:
  0.0 133.9 jit_solution(2540692978702080587)
XLA Ops:
  0.0 0.0 copy-start
  0.0 1.4 %copy.17 = bf16[1408,256]{1,0:T(8,128)(2,1)S(1)} copy(bf16[1408,256]{0,1:T(8,128)(2,1)} %bitcast.18) | data formatting | bytes 1441792 | tf_op jit(solution)/shard_map/transpose | solution.py:563
  1.5 1.4 %copy.18 = bf16[1408,256]{1,0:T(8,128)(2,1)S(1)} copy(bf16[1408,256]{0,1:T(8,128)(2,1)} %bitcast.19) | data formatting | bytes 1441792 | tf_op jit(solution)/shard_map/transpose | solution.py:564
  2.8 0.0 copy-done
  2.9 1.5 %pad_maximum_fusion.w_ref = bf16[4,1056,256]{2,1,0:T(8,128)(2,1)} fusion(bf16[4,352,256]{2,1,0:T(8,128)(2,1)S(1)} %bitcast.20, bf16[4,352,256]{2,1,0:T(8,128)(2,1)S(1)} %bitcast.17, bf16[4,352,256]{2,1,0:T(8,128)(2,1)S(1)} %bitcast.16), kind=kLoop, calls=%fused_computation | loop fusion | flops 6488064 | bytes 4325376 | tf_op jit(solution)/shard_map/concatenate | solution.py:561
  4.3 127.9 %layer.1 = bf16[64,2048]{1,0:T(8,128)(2,1)} custom-call(bf16[256,128]{1,0:T(8,128)(2,1)} %drive_ref.1, f32[8,256]{1,0:T(8,128)} %bitcast.25, f32[8,64]{1,0:T(8,128)} %decay_ref.1, f32[8,64]{1,0:T(8,128)} %turn_ref.1, f32[128,64]{1,0:T(8,128)} %bitcast.21, f32[128,64]{1,0:T(8,128)} %bitcast.22, f32[128,64]{1,0:T(8,128)} %bitcast.23, f32[128,64]{1,0:T(8,128)} %bitcast.24, ...), custom_call_target="tpu_custom_call" | custom-call | tf_op jit(solution)/shard_map/layer/pallas_call | solution.py:574
  132.3 1.7 %copy.20 = bf16[64,2048]{1,0:T(8,128)(2,1)} copy(bf16[64,2048]{1,0:T(8,128)(2,1)} %layer.1) | data formatting | bytes 524288
Async XLA Ops:
  0.0 2.8 %copy-start = (bf16[1408,256]{1,0:T(8,128)(2,1)S(1)}, bf16[1408,256]{1,0:T(8,128)(2,1)}, u32[]{:S(2)}) copy-start(bf16[1408,256]{1,0:T(8,128)(2,1)} %param.31) | copy-start | bytes 2162692
